TPU v7x, 256 devices: a whole 4x4x8 slice. The times are simulated.
256 devices in a mesh: ep: 32 (over z, x), tp: 8 (over y, core).
Axes of the slice: x: 4, y: 4, z: 8, core: 2. Of those that a mesh axis runs over, the one named last changes fastest.
Arguments:
- queries: bfloat16 [32768, 2048], P('ep', 'tp'), may hold values from -6 to 6
- key_vectors: bfloat16 [32768, 2048], P('ep', 'tp'), may hold values from -6 to 6
- value_vectors: bfloat16 [32768, 4096], P('ep', 'tp'), may hold values from -6 to 6
- decay_logit: float32 [32768, 2048], P('ep', 'tp'), may hold values from -11 to 16
- head_gain: float32 [256], replicated, may hold values from 0.1 to 1.9
- routed_rows: bfloat16 [8192, 4096], P('ep'), may hold values from -6 to 6
- pre_gain: float32 [4096], replicated, may hold values from 0.1 to 1.9
- expert_pick: int32 [8192, 2], P('ep'), may hold values from 0 to 31, as said below
- route_weight: float32 [8192, 2], P('ep'), may hold values from 0.2 to 1
- gate_weight: bfloat16 [32, 4096, 2048], P('ep', None, 'tp'), may hold values from -0.09375 to 0.09375
- up_weight: bfloat16 [32, 4096, 2048], P('ep', None, 'tp'), may hold values from -0.09375 to 0.09375
- down_weight: bfloat16 [32, 2048, 4096], P('ep', 'tp'), may hold values from -0.125 to 0.125
- post_gain: float32 [4096], replicated, may hold values from 0.1 to 1.9
Outputs:
- mixed_heads: bfloat16 [32768, 4096], P('ep', 'tp')
- routed_out: bfloat16 [8192, 4096], P(('ep', 'tp'))
Inputs may be any that keep to these rules, and one draw needn't show every extreme that they name: `expert_pick`: each row names 2 different experts, both in the same one of 4 equal groups of consecutive expert numbers. In every aligned block of 32 rows no expert is named more than 4 times, and some expert exactly 4 times.
All inputs are finite; a program needn't handle non-finite values.
Results may differ from a plain program's by a relative error of at most 0.015.
Values may be sent and summed in bfloat16 or wider, within the bound.
A program may use at most 128 MiB of HBM per device.

v0:
```python
import jax
import jax.numpy as jnp
from jax import lax
from jax.sharding import Mesh
from jax.sharding import PartitionSpec as P

DK = 128
DV = 256
BLK = 64
EP = ("ep_0", "ep_1")
EP_TP = ("ep_0", "ep_1", "tp")


def neutral_like(x, identity):
    return jax.tree.map(
        lambda part, zero: jnp.zeros_like(part) + jnp.asarray(zero, part.dtype), x, identity
    )


def prefix_by_axis(x, axes, combine, identity):
    before = start = neutral_like(x, identity)
    running = x
    for axis in reversed(axes):
        length, index = (lax.axis_size(axis), lax.axis_index(axis))
        pieces = jax.tree.map(
            lambda part, kind: lax.all_gather(part.astype(kind), axis),
            running,
            (jnp.bfloat16, jnp.bfloat16),
        )
        inside, running = (start, start)
        for k in range(length):
            passed = k < index
            running = combine(
                running, jax.tree.map(lambda part, own: part[k].astype(own.dtype), pieces, x)
            )
            inside = jax.tree.map(lambda new, old: jnp.where(passed, new, old), running, inside)
        before = combine(inside, before)
    return before


def chain_join(earlier, later_part):
    decay_first, initial_memory_matrix = earlier
    decay_second, state_second = later_part
    return (
        decay_first * decay_second,
        initial_memory_matrix * decay_second[..., None] + state_second,
    )


def row_norm(values, gain):
    return values * lax.rsqrt(jnp.mean(values * values, axis=-1, keepdims=True) + 1e-06) * gain


def token_mixer(queries, key_vectors, value_vectors, decay_logit, head_gain):
    blocks = queries.shape[0] // BLK
    heads_here = queries.shape[1] // DK
    key_shape = (blocks, BLK, heads_here, DK)
    log_rate = jax.nn.log_sigmoid(decay_logit).reshape(key_shape) / 16.0
    cumulative = jnp.cumsum(log_rate, axis=1)
    ending = cumulative[:, -1]
    query_rows = queries.reshape(key_shape)
    key_rows = key_vectors.reshape(key_shape)
    value_rows = value_vectors.reshape(blocks, BLK, heads_here, DV)
    query_decay = (query_rows * jnp.exp(cumulative)).astype(jnp.bfloat16)
    key_decay = (key_rows * jnp.exp(-cumulative)).astype(jnp.bfloat16)
    key_to_end = (key_rows * jnp.exp(ending[:, None] - cumulative)).astype(jnp.bfloat16)
    update = jnp.einsum(
        "njhd,njhe->nhde", key_to_end, value_rows, preferred_element_type=jnp.float32
    )
    step_decay = jnp.exp(ending)

    def advance(carry, inputs):
        carry_state, carry_decay = carry
        block_update, block_decay = inputs
        next_carry = (
            carry_state * block_decay[..., None] + block_update,
            carry_decay * block_decay,
        )
        return (next_carry, (carry_state, carry_decay))

    start_carry = (jnp.zeros_like(update[0]), jnp.ones_like(step_decay[0]))
    (final_state, total_decay), (local_states, local_decay) = lax.scan(
        advance, start_carry, (update, step_decay)
    )
    incoming = prefix_by_axis(
        (total_decay, final_state),
        EP,
        chain_join,
        (jnp.ones_like(total_decay), jnp.zeros_like(final_state)),
    )
    causal_mask = jnp.tril(jnp.ones((BLK, BLK), dtype=bool))
    scores = jnp.einsum(
        "nihd,njhd->nhij", query_decay, key_decay, preferred_element_type=jnp.float32
    )
    weights = jnp.where(causal_mask, scores, 0.0).astype(jnp.bfloat16)
    inside = jnp.einsum("nhij,njhe->nihe", weights, value_rows, preferred_element_type=jnp.float32)
    states = (local_states + incoming[1][None] * local_decay[..., None]).astype(jnp.bfloat16)
    carried = jnp.einsum("nihd,nhde->nihe", query_decay, states, preferred_element_type=jnp.float32)
    outputs = row_norm(inside + carried, head_gain).astype(jnp.bfloat16)
    return outputs.reshape(queries.shape[0], heads_here * DV)


def routed_experts(
    routed_rows, pre_gain, expert_pick, route_weight, gate_weight, up_weight, down_weight, post_gain
):
    tp_count = lax.axis_size("tp")
    ep_count = lax.axis_size(EP)
    part_index = lax.axis_index("tp")
    ep_rows, model_width = routed_rows.shape
    part_rows = ep_rows // tp_count
    top_count = expert_pick.shape[1]
    experts = ep_count * gate_weight.shape[0]
    capacity = 2 * top_count * part_rows // experts
    normed = row_norm(routed_rows.astype(jnp.float32), pre_gain).astype(jnp.bfloat16)
    padded = jnp.concatenate([normed, jnp.zeros((1, model_width), jnp.bfloat16)], axis=0)
    picks = expert_pick.reshape(tp_count, part_rows * top_count)
    matches = (picks[:, :, None] == jnp.arange(experts, dtype=jnp.int32)[None, None, :]).astype(
        jnp.int32
    )
    slots = jnp.sum((jnp.cumsum(matches, axis=1) - 1) * matches, axis=2)
    targets = picks * capacity + slots
    sources = (
        jnp.arange(part_rows * top_count, dtype=jnp.int32)[None, :] // top_count
        + part_rows * jnp.arange(tp_count, dtype=jnp.int32)[:, None]
    )
    slice_offset_index = jnp.broadcast_to(
        jnp.arange(tp_count, dtype=jnp.int32)[:, None], targets.shape
    )
    table = (
        jnp.full((tp_count, experts * capacity), ep_rows, jnp.int32)
        .at[slice_offset_index, targets]
        .set(sources)
    )
    gate_local = gate_weight[0]
    up_local = up_weight[0]
    down_local = down_weight[0]
    own_table = lax.dynamic_slice_in_dim(table, part_index, 1, 0)
    outgoing = padded[own_table].reshape(1, ep_count, capacity, model_width)
    arrived = lax.all_gather(
        lax.all_to_all(outgoing, EP, split_axis=1, concat_axis=1, tiled=True),
        "tp",
        axis=0,
        tiled=True,
    )
    gate_act = jnp.einsum("pskd,df->pskf", arrived, gate_local, preferred_element_type=jnp.float32)
    up_act = jnp.einsum("pskd,df->pskf", arrived, up_local, preferred_element_type=jnp.float32)
    hidden = (jax.nn.silu(gate_act) * up_act).astype(jnp.bfloat16)
    summed = lax.psum_scatter(
        jnp.einsum("pskf,fd->pskd", hidden, down_local, preferred_element_type=jnp.float32).astype(
            jnp.bfloat16
        ),
        "tp",
        scatter_dimension=0,
        tiled=True,
    )
    returned = lax.all_to_all(summed, EP, split_axis=1, concat_axis=1, tiled=True)
    flattened = returned.reshape(experts * capacity, model_width)
    my_slots = lax.dynamic_slice_in_dim(targets, part_index, 1, 0).reshape(part_rows, top_count)
    my_weight = lax.dynamic_slice_in_dim(route_weight, part_index * part_rows, part_rows, 0)
    combined = jnp.sum(flattened[my_slots].astype(jnp.float32) * my_weight[:, :, None], axis=1)
    return row_norm(combined, post_gain).astype(jnp.bfloat16)


def on_device(
    queries,
    key_vectors,
    value_vectors,
    decay_logit,
    head_gain,
    routed_rows,
    pre_gain,
    expert_pick,
    route_weight,
    gate_weight,
    up_weight,
    down_weight,
    post_gain,
):
    mixed_heads = token_mixer(queries, key_vectors, value_vectors, decay_logit, head_gain)
    routed_out = routed_experts(
        routed_rows,
        pre_gain,
        expert_pick,
        route_weight,
        gate_weight,
        up_weight,
        down_weight,
        post_gain,
    )
    return (mixed_heads, routed_out)


def solution(mesh):
    torus = Mesh(mesh.devices.reshape(8, 4, mesh.shape["tp"]), ("ep_0", "ep_1", "tp"))
    placed = (
        P(EP, "tp"),
        P(EP, "tp"),
        P(EP, "tp"),
        P(EP, "tp"),
        P(),
        P(EP, None),
        P(),
        P(EP, None),
        P(EP, None),
        P(EP, None, "tp"),
        P(EP, None, "tp"),
        P(EP, "tp", None),
        P(),
    )
    return jax.shard_map(
        on_device,
        mesh=torus,
        in_specs=placed,
        out_specs=(P(EP, "tp"), P(EP_TP, None)),
        check_vma=False,
    )
```

profile of v0, /device:TPU:2, one launch (start us, length us, event | category | flops | bytes accessed | tf_op | source)
XLA Modules:
  0.0 290.8 jit_solution(14638093598080471657)
XLA Ops:
  11.9 22.1 %scatter_fusion = s32[8,128]{1,0:T(8,128)S(1)} fusion(s32[8,128]{1,0:T(8,128)S(1)} %broadcast_in_dim.33, s32[512]{0:T(512)S(1)} %reshape.309, s32[512]{0:T(512)S(1)} %reshape.311), kind=kCustom, calls=%fused_computation.2 | custom fusion | bytes 10240 | tf_op jit(solution)/shard_map/scatter | solution.py:132
  34.0 2.1 fusion.1
  36.1 2.2 fusion.3
  39.9 4.1 %gather_fusion = bf16[128,4096]{1,0:T(8,128)(2,1)S(1)} fusion(bf16[257,4096]{1,0:T(8,128)(2,1)} %concatenate.6, s32[1024]{0:T(1024)S(1)} %pad_clamp_fusion.1), kind=kCustom, calls=%fused_computation | custom fusion | bytes 2097664 | tf_op jit(solution)/shard_map/gather | solution.py:138
  45.2 39.7 %all_to_all.10 = bf16[1,32,4,4096]{3,2,0,1:T(4,128)(2,1)S(1)} all-to-all(bf16[1,32,4,4096]{3,2,0,1:T(4,128)(2,1)} %bitcast.178), channel_id=1, replica_groups=mesh['ep_0'=8,'ep_1'=4,'tp'=8] {'ep_0','ep_1'}, dimensions={1} | all-to-all | bytes 2097152 | tf_op jit(solution)/shard_map/all_to_all | solution.py:140
  90.1 2.5 reshape.280
  92.6 2.6 reshape.281
  98.1 4.2 %multiply_convert_fusion.2 = (bf16[16,64,2,128]{3,0,1,2:T(8,128)(2,1)}, bf16[16,64,2,128]{3,0,1,2:T(8,128)(2,1)S(1)}, bf16[16,64,2,128]{3,0,1,2:T(8,128)(2,1)}) fusion(f32[16,64,2,128]{3,0,1,2:T(8,128)S(1)} %fusion.22, f32[16,64,2,128]{3,2,1,0:T(2,128)} %reshape.281, f32[16,2,128]{2,0,1:T(8,128)S(1)} %slice_bitcast_fusion.4, f32[16,64,2,128]{3,2,1,0:T(2,128)} %reshape.280), kind=kLoop, calls=%fused_computation.40 | loop fusion | flops 2097152 | bytes 4734976 | tf_op jit(solution)/shard_map/convert_element_type | solution.py:65
  102.3 2.7 fusion.24
  105.0 30.8 %all-gather.8.cloned.1.call-done = bf16[8,32,4,4096]{3,1,2,0:T(8,128)(2,1)} async-done(((bf16[1,32,4,4096]{3,1,2,0:T(8,128)(2,1)}), bf16[8,32,4,4096]{3,1,2,0:T(8,128)(2,1)}) %all-gather.8.cloned.1.call-update) | async-done | bytes 8388624 | tf_op jit(solution)/shard_map/all_gather | solution.py:139
  135.8 6.5 %fusion.8 = f32[8,32,4,256]{3,1,2,0:T(8,128)S(1)} fusion(bf16[8,32,4,4096]{3,1,2,0:T(8,128)(2,1)} %all-gather.8.cloned.1.call-done, bf16[1,4096,256]{2,1,0:T(8,128)(2,1)} %param.24), kind=kOutput, calls=%fused_computation.21 | convolution fusion | flops 2147483648 | bytes 11534336 | tf_op jit(solution)/shard_map/pskd,df->pskf/dot_general | solution.py:145
  142.7 2.4 fusion.15
  145.1 5.6 %convolution_convert_fusion = bf16[8,32,4,4096]{3,1,2,0:T(8,128)(2,1)} fusion(bf16[8,32,4,256]{3,1,2,0:T(8,128)(2,1)S(1)} %fusion.15, bf16[1,256,4096]{2,1,0:T(8,128)(2,1)S(1)} %copy-done), kind=kOutput, calls=%fused_computation.9 | convolution fusion | flops 2151677952 | bytes 11010048 | tf_op jit(solution)/shard_map/pskf,fd->pskd/dot_general | solution.py:149
  150.8 29.7 %while.17 = (s32[]{:T(128)}, f32[2,128,256]{2,1,0:T(8,128)S(1)}, f32[2,128]{1,0:T(2,128)S(1)}, f32[16,2,128,256]{3,2,1,0:T(8,128)}, f32[16,2,128]{2,1,0:T(2,128)...) while((s32[]{:T(128)}, f32[2,128,256]{2,1,0:T(8,128)S(1)}, ...), condition=%wide.region_2.3_spmd.clone, body=%wide.region_1.2_spmd.clone.sunk | while | flops 262915 | bytes 1319542 | solution.py:82
  180.6 7.8 %all-gather.2 = bf16[4,2,128]{2,1,0:T(2,128)(2,1)S(1)} all-gather(bf16[1,2,128]{2,1,0:T(2,128)(2,1)S(1)} %convert_bitcast_fusion.1), channel_id=2, replica_groups=mesh['ep_0'=8,'ep_1'=4,'tp'=8] {'ep_1'}, dimensions={0}, use_global_device_ids=true | all-gather | bytes 2560 | tf_op jit(solution)/shard_map/all_gather | solution.py:26
  188.4 12.2 %all-gather.1 = bf16[8,128,256]{2,1,0:T(8,128)(2,1)S(1)} all-gather(bf16[2,128,256]{2,1,0:T(8,128)(2,1)S(1)} %convert_element_type.277), channel_id=3, replica_groups=mesh['ep_0'=8,'ep_1'=4,'tp'=8] {'ep_1'}, dimensions={0}, use_global_device_ids=true | all-gather | bytes 655360 | tf_op jit(solution)/shard_map/all_gather | solution.py:26
  202.6 3.5 %reduce-scatter.2.cloned.1.call-done = bf16[1,32,4,4096]{3,1,2,0:T(8,128)(2,1)} async-done(((bf16[8,32,4,4096]{3,1,2,0:T(8,128)(2,1)}), bf16[1,32,4,4096]{3,1,2,0:T(8,128)(2,1)}) %reduce-scatter.2.cloned.1.call-update) | async-done | bytes 1048592 | tf_op jit(solution)/shard_map/reduce_scatter | solution.py:148
  206.1 3.0 %copy.101 = bf16[1,32,4,4096]{3,2,0,1:T(4,128)(2,1)} copy(bf16[1,32,4,4096]{3,1,2,0:T(8,128)(2,1)} %reduce-scatter.2.cloned.1.call-done) | data formatting | bytes 2097152 | tf_op jit(solution)/shard_map/reduce_scatter | solution.py:148
  209.1 10.2 %all-to-all-start.1 = ((bf16[1,32,4,4096]{3,2,0,1:T(4,128)(2,1)}), bf16[1,32,4,4096]{3,2,0,1:T(4,128)(2,1)}, u32[]{:S(2)}, u32[]{:S(2)}) async-start(bf16[1,32,4,4096]{3,2,0,1:T(4,128)(2,1)} %copy.101), calls=%async_computation.2 | async-start | bytes 2097152 | tf_op jit(solution)/shard_map/all_to_all | solution.py:156
  219.5 41.7 %all_gather.25 = bf16[8,2,128]{2,1,0:T(2,128)(2,1)S(1)} all-gather(bf16[1,2,128]{2,1,0:T(2,128)(2,1)S(1)} %get-tuple-element.129), channel_id=1, replica_groups=mesh['ep_0'=8,'ep_1'=4,'tp'=8] {'ep_0'}, dimensions={0}, use_global_device_ids=true | all-gather | bytes 4608 | tf_op jit(solution)/shard_map/all_gather | solution.py:26
  261.2 2.0 fusion.42
  263.2 4.7 %fusion.4 = f32[16,2,256,64]{2,3,1,0:T(8,128)} fusion(f32[16,2,128,256]{3,2,1,0:T(8,128)} %get-tuple-element.42, f32[16,2,128]{2,1,0:T(2,128)S(1)} %get-tuple-element.45, f32[2,128,256]{2,1,0:T(8,128)S(1)} %fusion.42, bf16[16,64,2,128]{3,0,1,2:T(8,128)(2,1)} %get-tuple-element.121), kind=kOutput, calls=%fused_computation.17 | convolution fusion | flops 137363456 | bytes 7094272 | tf_op jit(solution)/shard_map/nihd,nhde->nihe/dot_general | solution.py:98
  267.9 4.0 %multiply_reduce_fusion = (f32[16,64,2]{1,2,0:T(2,128)S(1)}, f32[16,64,2,256]{3,1,2,0:T(8,128)}) fusion(f32[16,2,256,64]{2,3,1,0:T(8,128)} %fusion.4, bf16[16,64,2,256]{3,2,1,0:T(2,128)(2,1)S(1)} %reshape.275, bf16[16,64,2,128]{3,0,1,2:T(8,128)(2,1)} %get-tuple-element.119, pred[64,64]{1,0:T(8,128)(4,1)S(1)} %iota_compare_fusion.3, ...), kind=kOutput, calls=%fused_computation.25 | convolution fusion | flops 102496256 | bytes 6303744 | tf_op jit(solution)/shard_map/nhij,njhe->nihe/dot_general | solution.py:96
  271.9 1.9 multiply_convert_fusion
  (163 shorter events, 56.0 us)
Async XLA Ops:
  8.0 137.1 %copy-start = (bf16[1,256,4096]{2,1,0:T(8,128)(2,1)S(1)}, bf16[1,256,4096]{2,1,0:T(8,128)(2,1)}, u32[]{:S(2)}) copy-start(bf16[1,256,4096]{2,1,0:T(8,128)(2,1)} %param.26) | copy-start | bytes 6291460
  8.0 127.8 %all-gather.8.cloned.1.call-start = ((), (), s32[]{:S(2)}) async-start(), calls=%async_computation.4 | async-start | bytes 9437184 | tf_op jit(solution)/shard_map/all_gather | solution.py:139
  11.9 24.2 %copy-start.2 = (f32[4096]{0:T(1024)S(1)}, f32[4096]{0:T(1024)}, u32[]{:S(2)}) copy-start(f32[4096]{0:T(1024)} %param.21) | copy-start | bytes 49156
  86.5 119.6 %reduce-scatter.2.cloned.1.call-start = ((), (), s32[]{:S(2)}) async-start(), calls=%async_computation.5 | async-start | bytes 9437184 | tf_op jit(solution)/shard_map/reduce_scatter | solution.py:148
  135.8 6.5 %copy-start.6 = (bf16[8,32,4,4096]{3,1,2,0:T(8,128)(2,1)S(1)}, bf16[8,32,4,4096]{3,1,2,0:T(8,128)(2,1)}, u32[]{:S(2)}) copy-start(bf16[8,32,4,4096]{3,1,2,0:T(8,128)(2,1)} %all-gather.8.cloned.1.call-done) | copy-start | bytes 25165828
  135.8 7.0 %copy-start.7 = (bf16[1,4096,256]{2,1,0:T(8,128)(2,1)S(1)}, bf16[1,4096,256]{2,1,0:T(8,128)(2,1)}, u32[]{:S(2)}) copy-start(bf16[1,4096,256]{2,1,0:T(8,128)(2,1)} %param.25) | copy-start | bytes 6291460
  150.7 110.5 %all-gather.6.cloned.1.call-start = ((), (), s32[]{:S(2)}) async-start(), calls=%async_computation.3 | async-start | bytes 1179648 | tf_op jit(solution)/shard_map/all_gather | solution.py:26
  180.5 38.8 %copy-start.5 = (f32[256,2]{0,1:T(2,128)S(1)}, f32[256,2]{0,1:T(2,128)}, u32[]{:S(2)}) copy-start(f32[256,2]{0,1:T(2,128)} %param.23) | copy-start | bytes 6148
  200.6 0.8 copy-start.1
  209.1 67.0 %all-to-all-start.1 = ((bf16[1,32,4,4096]{3,2,0,1:T(4,128)(2,1)}), bf16[1,32,4,4096]{3,2,0,1:T(4,128)(2,1)}, u32[]{:S(2)}, u32[]{:S(2)}) async-start(bf16[1,32,4,4096]{3,2,0,1:T(4,128)(2,1)} %copy.101), calls=%async_computation.2 | async-start | bytes 2097152 | tf_op jit(solution)/shard_map/all_to_all | solution.py:156
  267.9 4.0 %copy-start.4 = (f32[256]{0:T(256)S(1)}, f32[256]{0:T(256)}, u32[]{:S(2)}) copy-start(f32[256]{0:T(256)} %param.19) | copy-start | bytes 3076
  277.5 5.0 %copy-start.3 = (f32[4096]{0:T(1024)S(1)}, f32[4096]{0:T(1024)}, u32[]{:S(2)}) copy-start(f32[4096]{0:T(1024)} %param.27) | copy-start | bytes 49156
Sparse Core Ops, SparseCore 0:
  86.6 49.1 all-gather.7
  150.8 55.2 reduce-scatter.1
Sparse Core Ops, SparseCore 1:
  202.3 48.2 all-gather.5
where the time goes:
time: 292 us; the launch traced here: 291 us
  blocking collectives  101 us (35%)
  local copies, waits for them, and re-layouts  52.2 us (18%)
  other arithmetic  50.2 us (17%)
  waiting for transfers between devices  34.3 us (12%)
  matrix products  25.8 us (9%)
  between operations  15.9 us (5%)
  starting transfers between devices  10.5 us (4%)
    all_gather x3, blocking collectives, prefix_by_axis(): lax.all_gather(part.astype(kind), axis)  61.7 us
    all_to_all x1, blocking collectives, routed_experts(): lax.all_to_all(outgoing, EP, split_axis=1, concat_axis=1, tiled=True)  39.7 us
    all_gather x1, waiting for transfers between devices, routed_experts(): lax.all_gather(lax.all_to_all(outgoing, EP, split_axis=1, concat_axis=1,...  30.8 us
    scatter x1, local copies, waits for them, and re-layouts, routed_experts(): table = jnp.full((tp_count, experts * capacity), ep_rows, jnp.int32).at[s...  22.1 us
    add x16, other arithmetic, advance(): carry_state * block_decay[..., None] + block_update  17.1 us
    dynamic_update_slice x32, other arithmetic, token_mixer(): lax.scan(advance, start_carry, (update, step_decay))  11.8 us
    all_to_all x1, starting transfers between devices, routed_experts(): lax.all_to_all(summed, EP, split_axis=1, concat_axis=1, tiled=True)  10.2 us
    dot_general x1, matrix products, routed_experts(): jnp.einsum('pskd,df->pskf', arrived, gate_local, preferred_element_type=j...  6.46 us
  transfers between devices with their start and end apart: 4, of which 2 were waited for; matrix products, arithmetic and copies ran while one was open for 23% of the time, Pallas kernels for 0%

commit v1 on v0

--- a/solution.py
+++ b/solution.py
@@ -136,12 +136,9 @@
     down_local = down_weight[0]
     own_table = lax.dynamic_slice_in_dim(table, part_index, 1, 0)
     outgoing = padded[own_table].reshape(1, ep_count, capacity, model_width)
-    arrived = lax.all_gather(
-        lax.all_to_all(outgoing, EP, split_axis=1, concat_axis=1, tiled=True),
-        "tp",
-        axis=0,
-        tiled=True,
-    )
+    block = lax.all_to_all(outgoing, EP, split_axis=1, concat_axis=1, tiled=True)
+    stack = jnp.stack([block] * lax.axis_size("tp"))
+    arrived = jnp.concatenate(lax.all_to_all(stack, "tp", 0, 0), axis=0)
     gate_act = jnp.einsum("pskd,df->pskf", arrived, gate_local, preferred_element_type=jnp.float32)
     up_act = jnp.einsum("pskd,df->pskf", arrived, up_local, preferred_element_type=jnp.float32)
     hidden = (jax.nn.silu(gate_act) * up_act).astype(jnp.bfloat16)

time: 292 us -> 343 us (1.17)
  waiting for transfers between devices: 34.3 us -> 74.2 us
  local copies, waits for them, and re-layouts: 52.2 us -> 56 us
    all_to_all x0 -> x1, waiting for transfers between devices: none -> 74.1 us  [routed_experts(): arrived = jnp.concatenate(lax.all_to_all(stack, 'tp', 0, 0), axis=0)]
    all_gather x1 -> x0, waiting for transfers between devices: 30.8 us -> none  [routed_experts(): lax.all_gather(lax.all_to_all(outgoing, EP, split_axis=1, concat_axis=1,...]
    all_to_all x0 -> x1, starting transfers between devices: none -> 4.96 us  [routed_experts(): arrived = jnp.concatenate(lax.all_to_all(stack, 'tp', 0, 0), axis=0)]
    another operation x0 -> x1, local copies, waits for them, and re-layouts: none -> 4.26 us  [routed_experts(): stack = jnp.stack([block] * lax.axis_size('tp'))]
    reduce_scatter x1, waiting for transfers between devices: 3.47 us -> 0.02 us  [routed_experts(): lax.psum_scatter(jnp.einsum('pskf,fd->pskd', hidden, down_local, preferre...]
  transfers between devices with their start and end apart: 4 -> 4, of which waited for: 2 -> 1; matrix products, arithmetic and copies ran while one was open for 23% -> 20% of each run, Pallas kernels for 0% -> 0%
where the time goes in v1:
time: 343 us; the launch traced here: 342 us
  blocking collectives  101 us (29%)
  waiting for transfers between devices  74.2 us (22%)
  local copies, waits for them, and re-layouts  56 us (16%)
  other arithmetic  51.3 us (15%)
  matrix products  29.2 us (9%)
  between operations  15.9 us (5%)
  starting transfers between devices  13.3 us (4%)
    all_to_all x1, waiting for transfers between devices, routed_experts(): arrived = jnp.concatenate(lax.all_to_all(stack, 'tp', 0, 0), axis=0)  74.1 us
    all_gather x3, blocking collectives, prefix_by_axis(): lax.all_gather(part.astype(kind), axis)  61.6 us
    all_to_all x1, blocking collectives, routed_experts(): lax.all_to_all(outgoing, EP, split_axis=1, concat_axis=1, tiled=True)  39.7 us
    scatter x1, local copies, waits for them, and re-layouts, routed_experts(): table = jnp.full((tp_count, experts * capacity), ep_rows, jnp.int32).at[s...  22.1 us
    add x16, other arithmetic, advance(): carry_state * block_decay[..., None] + block_update  17.1 us
    dynamic_update_slice x32, other arithmetic, token_mixer(): lax.scan(advance, start_carry, (update, step_decay))  11.9 us
    all_to_all x1, starting transfers between devices, routed_experts(): lax.all_to_all(summed, EP, split_axis=1, concat_axis=1, tiled=True)  8.08 us
  transfers between devices with their start and end apart: 4, of which 1 were waited for; matrix products, arithmetic and copies ran while one was open for 20% of the time, Pallas kernels for 0%

profile of v1, /device:TPU:2, one launch (start us, length us, event | category | flops | bytes accessed | tf_op | source)
XLA Modules:
  0.0 341.8 jit_solution(10895617428590153386)
XLA Ops:
  14.0 22.1 %scatter_fusion = s32[8,128]{1,0:T(8,128)S(1)} fusion(s32[8,128]{1,0:T(8,128)S(1)} %broadcast_in_dim.33, s32[512]{0:T(512)S(1)} %reshape.316, s32[512]{0:T(512)S(1)} %reshape.318), kind=kCustom, calls=%fused_computation.2 | custom fusion | bytes 10240 | tf_op jit(solution)/shard_map/scatter | solution.py:132
  36.1 2.2 fusion.7
  39.9 4.1 %gather_fusion = bf16[128,4096]{1,0:T(8,128)(2,1)S(1)} fusion(bf16[257,4096]{1,0:T(8,128)(2,1)} %concatenate.6, s32[1024]{0:T(1024)S(1)} %pad_clamp_fusion.1), kind=kCustom, calls=%fused_computation | custom fusion | bytes 2097664 | tf_op jit(solution)/shard_map/gather | solution.py:138
  45.2 39.7 %all_to_all.18 = bf16[1,32,4,4096]{3,2,0,1:T(4,128)(2,1)S(1)} all-to-all(bf16[1,32,4,4096]{3,2,0,1:T(4,128)(2,1)} %bitcast.187), channel_id=1, replica_groups=mesh['ep_0'=8,'ep_1'=4,'tp'=8] {'ep_0','ep_1'}, dimensions={1} | all-to-all | bytes 2097152 | tf_op jit(solution)/shard_map/all_to_all | solution.py:139
  85.5 4.3 %stack.2 = bf16[8,1,32,4,4096]{4,2,3,1,0:T(8,128)(2,1)} broadcast(bf16[32,4,4096]{2,0,1:T(8,128)(2,1)S(1)} %copy.101), dimensions={2,3,4} | broadcast | bytes 9437184 | tf_op jit(solution)/shard_map/stack | solution.py:140
  89.7 5.0 %all-to-all-start.1 = ((bf16[8,1,32,4,4096]{4,2,3,1,0:T(8,128)(2,1)}), bf16[8,1,32,4,4096]{4,2,3,1,0:T(8,128)(2,1)}, u32[]{:S(2)}, u32[]{:S(2)}) async-start(bf16[8,1,32,4,4096]{4,2,3,1,0:T(8,128)(2,1)} %stack.2), calls=%async_computation.1 | async-start | bytes 16777216 | tf_op jit(solution)/shard_map/all_to_all | solution.py:141
  96.3 2.6 reshape.287
  98.9 2.5 reshape.288
  101.4 2.8 fusion.26
  104.2 2.7 div.38
  108.3 4.1 %multiply_convert_fusion.2 = (bf16[16,64,2,128]{3,0,1,2:T(8,128)(2,1)}, bf16[16,64,2,128]{3,0,1,2:T(8,128)(2,1)S(1)}, bf16[16,64,2,128]{3,0,1,2:T(8,128)(2,1)}) fusion(f32[16,64,2,128]{3,0,1,2:T(8,128)S(1)} %fusion.28, f32[16,64,2,128]{3,2,1,0:T(2,128)} %reshape.288, f32[16,2,128]{2,0,1:T(8,128)S(1)} %slice_bitcast_fusion.4, f32[16,64,2,128]{3,2,1,0:T(2,128)} %reshape.287), kind=kLoop, calls=%fused_computation.42 | loop fusion | flops 2097152 | bytes 4734976 | tf_op jit(solution)/shard_map/convert_element_type | solution.py:65
  112.4 2.7 fusion.30
  115.1 74.1 %all-to-all-done.1 = bf16[8,1,32,4,4096]{4,2,3,1,0:T(8,128)(2,1)} async-done(((bf16[8,1,32,4,4096]{4,2,3,1,0:T(8,128)(2,1)}), bf16[8,1,32,4,4096]{4,2,3,1,0:T(8,128)(2,1)}, u32[]{:S(2)}, u32[]{:S(2)}) %all-to-all-start.1) | async-done | bytes 8388640 | tf_op jit(solution)/shard_map/all_to_all | solution.py:141
  189.3 6.5 %fusion.3 = f32[8,32,4,256]{3,1,2,0:T(8,128)S(1)} fusion(bf16[8,1,32,4,4096]{4,2,3,1,0:T(8,128)(2,1)} %all-to-all-done.1, bf16[1,4096,256]{2,1,0:T(8,128)(2,1)} %param.24), kind=kOutput, calls=%fused_computation.11 | convolution fusion | flops 2147483648 | bytes 11534336 | tf_op jit(solution)/shard_map/pskd,df->pskf/dot_general | solution.py:142
  195.8 5.8 %fusion.19 = bf16[8,32,4,256]{3,1,2,0:T(8,128)(2,1)S(1)} fusion(bf16[1,4096,256]{2,1,0:T(8,128)(2,1)S(1)} %copy-done.6, bf16[8,1,32,4,4096]{4,2,3,1,0:T(8,128)(2,1)} %all-to-all-done.1, f32[8,32,4,256]{3,1,2,0:T(8,128)S(1)} %fusion.3), kind=kOutput, calls=%fused_computation.32 | convolution fusion | flops 2149056512 | bytes 12058624 | tf_op jit(solution)/shard_map/pskd,df->pskf/dot_general | solution.py:143
  201.5 5.6 %convolution_convert_fusion = bf16[8,32,4,4096]{3,1,2,0:T(8,128)(2,1)} fusion(bf16[8,32,4,256]{3,1,2,0:T(8,128)(2,1)S(1)} %fusion.19, bf16[1,256,4096]{2,1,0:T(8,128)(2,1)S(1)} %copy-done), kind=kOutput, calls=%fused_computation.13 | convolution fusion | flops 2151677952 | bytes 11010048 | tf_op jit(solution)/shard_map/pskf,fd->pskd/dot_general | solution.py:146
  207.2 30.0 %while.17 = (s32[]{:T(128)}, f32[2,128,256]{2,1,0:T(8,128)S(1)}, f32[2,128]{1,0:T(2,128)S(1)}, f32[16,2,128,256]{3,2,1,0:T(8,128)}, f32[16,2,128]{2,1,0:T(2,128)...) while((s32[]{:T(128)}, f32[2,128,256]{2,1,0:T(8,128)S(1)}, ...), condition=%wide.region_2.3_spmd.clone, body=%wide.region_1.2_spmd.clone.sunk | while | flops 262915 | bytes 1319042 | solution.py:82
  237.2 7.8 %all-gather.2 = bf16[4,2,128]{2,1,0:T(2,128)(2,1)S(1)} all-gather(bf16[1,2,128]{2,1,0:T(2,128)(2,1)S(1)} %convert_bitcast_fusion.1), channel_id=2, replica_groups=mesh['ep_0'=8,'ep_1'=4,'tp'=8] {'ep_1'}, dimensions={0}, use_global_device_ids=true | all-gather | bytes 2560 | tf_op jit(solution)/shard_map/all_gather | solution.py:26
  245.1 12.2 %all-gather.1 = bf16[8,128,256]{2,1,0:T(8,128)(2,1)S(1)} all-gather(bf16[2,128,256]{2,1,0:T(8,128)(2,1)S(1)} %convert_element_type.277), channel_id=3, replica_groups=mesh['ep_0'=8,'ep_1'=4,'tp'=8] {'ep_1'}, dimensions={0}, use_global_device_ids=true | all-gather | bytes 655360 | tf_op jit(solution)/shard_map/all_gather | solution.py:26
  259.3 3.0 copy.102
  262.3 8.1 %all-to-all-start.2 = ((bf16[1,32,4,4096]{3,2,0,1:T(4,128)(2,1)}), bf16[1,32,4,4096]{3,2,0,1:T(4,128)(2,1)}, u32[]{:S(2)}, u32[]{:S(2)}) async-start(bf16[1,32,4,4096]{3,2,0,1:T(4,128)(2,1)} %copy.102), calls=%async_computation.3 | async-start | bytes 2097152 | tf_op jit(solution)/shard_map/all_to_all | solution.py:153
  270.6 41.6 %all_gather.22 = bf16[8,2,128]{2,1,0:T(2,128)(2,1)S(1)} all-gather(bf16[1,2,128]{2,1,0:T(2,128)(2,1)S(1)} %get-tuple-element.129), channel_id=1, replica_groups=mesh['ep_0'=8,'ep_1'=4,'tp'=8] {'ep_0'}, dimensions={0}, use_global_device_ids=true | all-gather | bytes 4608 | tf_op jit(solution)/shard_map/all_gather | solution.py:26
  314.2 4.7 %fusion.8 = f32[16,2,256,64]{2,3,1,0:T(8,128)} fusion(f32[16,2,128,256]{3,2,1,0:T(8,128)} %get-tuple-element.42, f32[16,2,128]{2,1,0:T(2,128)S(1)} %get-tuple-element.45, f32[2,128,256]{2,1,0:T(8,128)S(1)} %fusion.48, bf16[16,64,2,128]{3,0,1,2:T(8,128)(2,1)} %get-tuple-element.121), kind=kOutput, calls=%fused_computation.21 | convolution fusion | flops 137363456 | bytes 7094272 | tf_op jit(solution)/shard_map/nihd,nhde->nihe/dot_general | solution.py:98
  318.9 4.0 %multiply_reduce_fusion = (f32[16,64,2]{1,2,0:T(2,128)S(1)}, f32[16,64,2,256]{3,1,2,0:T(8,128)}) fusion(f32[16,2,256,64]{2,3,1,0:T(8,128)} %fusion.8, bf16[16,64,2,256]{3,2,1,0:T(2,128)(2,1)S(1)} %reshape.281, bf16[16,64,2,128]{3,0,1,2:T(8,128)(2,1)} %get-tuple-element.119, pred[64,64]{1,0:T(8,128)(4,1)S(1)} %iota_compare_fusion.3, ...), kind=kOutput, calls=%fused_computation.27 | convolution fusion | flops 102496256 | bytes 6303744 | tf_op jit(solution)/shard_map/nhij,njhe->nihe/dot_general | solution.py:96
  (161 shorter events, 57.2 us)
Async XLA Ops:
  8.0 193.5 %copy-start = (bf16[1,256,4096]{2,1,0:T(8,128)(2,1)S(1)}, bf16[1,256,4096]{2,1,0:T(8,128)(2,1)}, u32[]{:S(2)}) copy-start(bf16[1,256,4096]{2,1,0:T(8,128)(2,1)} %param.26) | copy-start | bytes 6291460
  14.0 22.1 %copy-start.2 = (f32[4096]{0:T(1024)S(1)}, f32[4096]{0:T(1024)}, u32[]{:S(2)}) copy-start(f32[4096]{0:T(1024)} %param.21) | copy-start | bytes 49156
  89.7 99.6 %all-to-all-start.1 = ((bf16[8,1,32,4,4096]{4,2,3,1,0:T(8,128)(2,1)}), bf16[8,1,32,4,4096]{4,2,3,1,0:T(8,128)(2,1)}, u32[]{:S(2)}, u32[]{:S(2)}) async-start(bf16[8,1,32,4,4096]{4,2,3,1,0:T(8,128)(2,1)} %stack.2), calls=%async_computation.1 | async-start | bytes 16777216 | tf_op jit(solution)/shard_map/all_to_all | solution.py:141
  94.7 164.6 %reduce-scatter.2.cloned.1.call-start = ((), (), s32[]{:S(2)}) async-start(), calls=%async_computation.5 | async-start | bytes 9437184 | tf_op jit(solution)/shard_map/reduce_scatter | solution.py:145
  189.3 6.5 %copy-start.6 = (bf16[1,4096,256]{2,1,0:T(8,128)(2,1)S(1)}, bf16[1,4096,256]{2,1,0:T(8,128)(2,1)}, u32[]{:S(2)}) copy-start(bf16[1,4096,256]{2,1,0:T(8,128)(2,1)} %param.25) | copy-start | bytes 6291460
  207.1 105.1 %all-gather.5.cloned.1.call-start = ((), (), s32[]{:S(2)}) async-start(), calls=%async_computation.4 | async-start | bytes 1179648 | tf_op jit(solution)/shard_map/all_gather | solution.py:26
  237.2 33.2 %copy-start.5 = (f32[256,2]{0,1:T(2,128)S(1)}, f32[256,2]{0,1:T(2,128)}, u32[]{:S(2)}) copy-start(f32[256,2]{0,1:T(2,128)} %param.23) | copy-start | bytes 6148
  257.2 0.8 copy-start.1
  262.3 64.8 %all-to-all-start.2 = ((bf16[1,32,4,4096]{3,2,0,1:T(4,128)(2,1)}), bf16[1,32,4,4096]{3,2,0,1:T(4,128)(2,1)}, u32[]{:S(2)}, u32[]{:S(2)}) async-start(bf16[1,32,4,4096]{3,2,0,1:T(4,128)(2,1)} %copy.102), calls=%async_computation.3 | async-start | bytes 2097152 | tf_op jit(solution)/shard_map/all_to_all | solution.py:153
  318.9 4.0 %copy-start.4 = (f32[256]{0:T(256)S(1)}, f32[256]{0:T(256)}, u32[]{:S(2)}) copy-start(f32[256]{0:T(256)} %param.19) | copy-start | bytes 3076
  328.5 5.0 %copy-start.3 = (f32[4096]{0:T(1024)S(1)}, f32[4096]{0:T(1024)}, u32[]{:S(2)}) copy-start(f32[4096]{0:T(1024)} %param.27) | copy-start | bytes 49156
Sparse Core Ops, SparseCore 0:
  207.2 49.8 reduce-scatter.1
Sparse Core Ops, SparseCore 1:
  259.0 43.1 all-gather.4
